TPU v7x, 256 devices: a whole 4x4x8 slice. The times are simulated.
256 devices in a mesh: sp: 32 (over z, y), tp: 8 (over x, core).
Axes of the slice: x: 4, y: 4, z: 8, core: 2. Of those that a mesh axis runs over, the one named last changes fastest.
Arguments:
- residual_in: bfloat16 [12288, 2048], P(('sp', 'tp')), may hold values from -6 to 6
- queries: bfloat16 [12288, 2048], P('sp', 'tp'), may hold values from -180 to 180
- keys: bfloat16 [12288, 2048], P('sp', 'tp'), may hold values from -9 to 9
- values: bfloat16 [12288, 2048], P('sp', 'tp'), may hold values from -6 to 6
- mix_lambda: float32 [16], P('tp'), may hold values from 0.3 to 0.8
- head_gain: float32 [128], replicated, may hold values from 0.1 to 1.9
- out_weight: bfloat16 [2048, 2048], P('tp'), may hold values from -0.125 to 0.125
- norm_gain: float32 [2048], replicated, may hold values from 0.1 to 1.9
- gate_weight: bfloat16 [2048, 5632], P('sp', 'tp'), may hold values from -0.125 to 0.125
- up_weight: bfloat16 [2048, 5632], P('sp', 'tp'), may hold values from -0.125 to 0.125
- down_weight: bfloat16 [5632, 2048], P('tp', 'sp'), may hold values from -0.078125 to 0.078125
Outputs:
- layer_out: bfloat16 [12288, 2048], P(('sp', 'tp'))
All inputs are finite; a program needn't handle non-finite values.
Results may differ from a plain program's by a relative error of at most 0.014.
Values may be sent and summed in bfloat16 or wider, within the bound.
No kernel may reach another device: no remote copies, remote signals or barrier semaphores. Data moves between devices by JAX's collectives and lax.ppermute only.
A program may use at most 128 MiB of HBM per device.

v0:
```python
import math
import jax
import jax.numpy as jnp
from jax import lax
from jax.sharding import PartitionSpec as P

DH = 64
VD = 128


def cut_along(value, dim, devices):
    shape = value.shape
    parts = value.reshape(*shape[:dim], devices, shape[dim] // devices, *shape[dim + 1 :])
    return jnp.moveaxis(parts, dim, 0)


def sent_and_summed(value, axis, dim):
    parts = cut_along(value, dim, lax.axis_size(axis))
    arrived = lax.all_to_all(parts, axis, split_axis=0, concat_axis=0, tiled=True)
    return arrived.astype(jnp.float32).sum(axis=0)


def sent_to_all(value, axis):
    copies = jnp.broadcast_to(value, (lax.axis_size(axis), *value.shape))
    return lax.all_to_all(copies, axis, split_axis=0, concat_axis=0, tiled=True)


def joined_along(parts, dim):
    shape = list(parts.shape[1:])
    shape[dim] *= parts.shape[0]
    return jnp.moveaxis(parts, 0, dim).reshape(shape)


def collect(value, axis, dim):
    parts = sent_to_all(value, axis)
    return joined_along(parts, dim)


def rows_first(arrays, axis, dims):
    turned = [jnp.moveaxis(a, dim, 0) for a, dim in zip(arrays, dims)]
    widths = [t[0].size for t in turned]
    both = jnp.concatenate([t.reshape(-1, w) for t, w in zip(turned, widths)], axis=1)
    result = lax.all_gather(both, axis, axis=0, tiled=True)
    parts = jnp.split(result, [sum(widths[:k]) for k in range(1, len(widths))], axis=1)
    return tuple(
        (
            jnp.moveaxis(b.reshape(-1, *t.shape[1:]), 0, dim)
            for b, t, dim in zip(parts, turned, dims)
        )
    )


def body(
    residual_in,
    queries,
    keys,
    values,
    mix_lambda,
    head_gain,
    out_weight,
    norm_gain,
    gate_weight,
    up_weight,
    down_weight,
):
    tok_local = queries.shape[0]
    heads_local = mix_lambda.shape[0]
    query_four = queries.reshape(tok_local, heads_local, 2, DH)
    inverse_root = 1.0 / math.sqrt(DH)

    def one_block(state, block):
        top, total, weighted = state
        key_block, value_block = block
        scores = (
            jnp.einsum("qhcd,khcd->hcqk", query_four, key_block, preferred_element_type=jnp.float32)
            * inverse_root
        )
        new_top = jnp.maximum(top, jnp.max(scores, axis=-1))
        rescale = jnp.exp(top - new_top)
        expo = jnp.exp(scores - new_top[..., None])
        total = total * rescale + jnp.sum(expo, axis=-1)
        weighted = weighted * rescale[..., None] + jnp.einsum(
            "hcqk,khe->hcqe",
            expo.astype(jnp.bfloat16),
            value_block,
            preferred_element_type=jnp.float32,
        )
        return ((new_top, total, weighted), None)

    start_state = (
        jnp.full((heads_local, 2, tok_local), -1e30, jnp.float32),
        jnp.zeros((heads_local, 2, tok_local), jnp.float32),
        jnp.zeros((heads_local, 2, tok_local, VD), jnp.float32),
    )
    key_piece = lax.all_gather(keys, "sp", axis=0, tiled=True)
    value_piece = lax.all_gather(values, "sp", axis=0, tiled=True)
    count = key_piece.shape[0]
    shards = max(count // tok_local, 1)
    unit = count // shards
    group = max(
        (g for g in range(1, shards + 1) if shards % g == 0 and g * unit <= max(1536, unit))
    )
    width = group * unit
    blocks = count // width
    key_blocks = key_piece.reshape(blocks, width, heads_local, 2, DH)
    value_blocks = value_piece.reshape(blocks, width, heads_local, VD)
    state, unused = lax.scan(one_block, start_state, (key_blocks, value_blocks))
    top, total, weighted = state
    maps = weighted / total[..., None]
    mixed = maps[:, 0] - mix_lambda[:, None, None] * maps[:, 1]
    head_scale = lax.rsqrt(jnp.mean(mixed * mixed, axis=-1, keepdims=True) + 1e-06)
    head_out = (mixed * head_scale * head_gain).astype(jnp.bfloat16)
    attended = jnp.transpose(head_out, (1, 0, 2)).reshape(tok_local, heads_local * VD)
    picked = attended
    projected = sent_and_summed(
        jnp.dot(picked, out_weight, preferred_element_type=jnp.float32).astype(jnp.bfloat16),
        "tp",
        0,
    )
    after_mix = residual_in.astype(jnp.float32) + projected
    row_scale = lax.rsqrt(jnp.mean(after_mix * after_mix, axis=-1, keepdims=True) + 1e-06)
    normed = (after_mix * row_scale * norm_gain).astype(jnp.bfloat16)
    all_rows = collect(normed, "tp", 0)
    gate_all, up_all, down_all = rows_first((gate_weight, up_weight, down_weight), "sp", (0, 0, 1))
    gate = jnp.dot(all_rows, gate_all, preferred_element_type=jnp.float32)
    up = jnp.dot(all_rows, up_all, preferred_element_type=jnp.float32)
    hidden = (jax.nn.silu(gate) * up).astype(jnp.bfloat16)
    picked = hidden
    mixer = sent_and_summed(
        jnp.dot(picked, down_all, preferred_element_type=jnp.float32).astype(jnp.bfloat16), "tp", 0
    )
    return (after_mix + 0.5 * mixer).astype(jnp.bfloat16)


def solution(mesh):
    return jax.shard_map(
        body,
        mesh=mesh,
        in_specs=(
            P(("sp", "tp"), None),
            P("sp", "tp"),
            P("sp", "tp"),
            P("sp", "tp"),
            P("tp"),
            P(),
            P("tp", None),
            P(),
            P("sp", "tp"),
            P("sp", "tp"),
            P("tp", "sp"),
        ),
        out_specs=P(("sp", "tp"), None),
        check_vma=False,
    )
```

profile of v0, /device:TPU:1, one launch (start us, length us, event | category | flops | bytes accessed | tf_op | source)
XLA Modules:
  0.0 425.4 jit_solution(3736161622382868444)
XLA Ops:
  6.5 0.7 all-gather.4.cloned.1.call-update
  7.3 0.7 all-gather.6.cloned.1.call-update
  8.1 1.9 concatenate.3
  10.0 1.1 copy.17
  11.1 89.9 %all-gather.4.cloned.1.call-done = bf16[12288,256]{1,0:T(8,128)(2,1)} async-done(((bf16[384,256]{1,0:T(8,128)(2,1)}), bf16[12288,256]{1,0:T(8,128)(2,1)}) %all-gather.4.cloned.1.call-update) | async-done | bytes 6291472 | tf_op jit(solution)/shard_map/all_gather | solution.py:95
  101.0 21.8 %reshape.51 = bf16[8,1536,2,2,64]{4,3,2,1,0:T(2,128)(2,1)} reshape(bf16[12288,256]{1,0:T(8,128)(2,1)} %all-gather.4.cloned.1.call-done) | data formatting | bytes 12582912 | tf_op jit(solution)/shard_map/reshape | solution.py:105
  122.8 29.8 %copy.19 = bf16[8,1536,2,2,64]{1,4,3,2,0:T(8,128)(2,1)} copy(bf16[8,1536,2,2,64]{4,3,2,1,0:T(2,128)(2,1)} %reshape.51) | data formatting | bytes 12582912
  152.6 36.1 %all-gather.6.cloned.1.call-done = bf16[12288,256]{1,0:T(8,128)(2,1)} async-done(((bf16[384,256]{1,0:T(8,128)(2,1)}), bf16[12288,256]{1,0:T(8,128)(2,1)}) %all-gather.6.cloned.1.call-update) | async-done | bytes 6291472 | tf_op jit(solution)/shard_map/all_gather | solution.py:96
  188.7 9.7 %reshape.52 = bf16[8,1536,2,128]{3,2,1,0:T(2,128)(2,1)} reshape(bf16[12288,256]{1,0:T(8,128)(2,1)} %all-gather.6.cloned.1.call-done) | data formatting | bytes 12582912 | tf_op jit(solution)/shard_map/reshape | solution.py:106
  198.5 128.2 %while.15 = (s32[]{:T(128)}, f32[2,2,384]{2,1,0:T(2,128)S(1)}, f32[2,2,384]{2,1,0:T(2,128)S(1)}, f32[2,2,384,128]{3,2,1,0:T(8,128)S(1)}, bf16[8,1536,2,2,64]{1,4...) while((s32[]{:T(128)}, f32[2,2,384]{2,1,0:T(2,128)S(1)}, ...), condition=%wide.region_3.4_spmd.clone, body=%wide.region_0.3_spmd.clone.sunk | while | flops 925441536 | bytes 71074440 | solution.py:107
  198.5 6.2 %bitcast_reduce_fusion.2 = (f32[2,2,384]{2,1,0:T(2,128)S(1)}, f32[2,2,1536,384]{3,2,1,0:T(8,128)}) fusion(bf16[384,2,2,64]{0,3,2,1:T(8,128)(2,1)S(1)} %get-tuple-element.168, bf16[8,1536,2,2,64]{1,4,3,2,0:T(8,128)(2,1)} %get-tuple-element.167, s32[]{:T(128)} %get-tuple-element.154), kind=kOutput, calls=%fused_computation.1.clone.1 | convolution fusion | flops 306706944 | bytes 10426880 | tf_op jit(solution)/shard_map/while/body/eval_jaxpr/qhcd,khcd->hcqk/dot_general | solution.py:75
  204.7 5.4 %fusion.55 = f32[2,2,384]{2,1,0:T(2,128)S(1)} fusion(f32[2,2,1536,384]{3,2,1,0:T(8,128)} %get-tuple-element.142, f32[2,2,384]{2,1,0:T(2,128)S(1)} %fusion.54), kind=kLoop, calls=%fused_computation.4.clone.1 | loop fusion | flops 7076352 | bytes 9449472 | tf_op jit(solution)/shard_map/while/body/eval_jaxpr/reduce_sum | solution.py:81
  210.2 1.6 constant_dynamic-slice_fusion.2
  211.8 2.6 fusion.57
  214.4 6.2 %bitcast_reduce_fusion.2 = (f32[2,2,384]{2,1,0:T(2,128)S(1)}, f32[2,2,1536,384]{3,2,1,0:T(8,128)}) fusion(bf16[384,2,2,64]{0,3,2,1:T(8,128)(2,1)S(1)} %get-tuple-element.168, bf16[8,1536,2,2,64]{1,4,3,2,0:T(8,128)(2,1)} %get-tuple-element.167, s32[]{:T(128)} %get-tuple-element.154), kind=kOutput, calls=%fused_computation.1.clone.1 | convolution fusion | flops 306706944 | bytes 10426880 | tf_op jit(solution)/shard_map/while/body/eval_jaxpr/qhcd,khcd->hcqk/dot_general | solution.py:75
  220.7 5.4 %fusion.55 = f32[2,2,384]{2,1,0:T(2,128)S(1)} fusion(f32[2,2,1536,384]{3,2,1,0:T(8,128)} %get-tuple-element.142, f32[2,2,384]{2,1,0:T(2,128)S(1)} %fusion.54), kind=kLoop, calls=%fused_computation.4.clone.1 | loop fusion | flops 7076352 | bytes 9449472 | tf_op jit(solution)/shard_map/while/body/eval_jaxpr/reduce_sum | solution.py:81
  226.1 1.6 constant_dynamic-slice_fusion.2
  227.7 2.6 fusion.57
  230.4 6.2 %bitcast_reduce_fusion.2 = (f32[2,2,384]{2,1,0:T(2,128)S(1)}, f32[2,2,1536,384]{3,2,1,0:T(8,128)}) fusion(bf16[384,2,2,64]{0,3,2,1:T(8,128)(2,1)S(1)} %get-tuple-element.168, bf16[8,1536,2,2,64]{1,4,3,2,0:T(8,128)(2,1)} %get-tuple-element.167, s32[]{:T(128)} %get-tuple-element.154), kind=kOutput, calls=%fused_computation.1.clone.1 | convolution fusion | flops 306706944 | bytes 10426880 | tf_op jit(solution)/shard_map/while/body/eval_jaxpr/qhcd,khcd->hcqk/dot_general | solution.py:75
  236.6 5.6 %fusion.55 = f32[2,2,384]{2,1,0:T(2,128)S(1)} fusion(f32[2,2,1536,384]{3,2,1,0:T(8,128)} %get-tuple-element.142, f32[2,2,384]{2,1,0:T(2,128)S(1)} %fusion.54), kind=kLoop, calls=%fused_computation.4.clone.1 | loop fusion | flops 7076352 | bytes 9449472 | tf_op jit(solution)/shard_map/while/body/eval_jaxpr/reduce_sum | solution.py:81
  242.2 1.9 constant_dynamic-slice_fusion.2
  244.1 2.6 fusion.57
  246.8 6.2 %bitcast_reduce_fusion.2 = (f32[2,2,384]{2,1,0:T(2,128)S(1)}, f32[2,2,1536,384]{3,2,1,0:T(8,128)}) fusion(bf16[384,2,2,64]{0,3,2,1:T(8,128)(2,1)S(1)} %get-tuple-element.168, bf16[8,1536,2,2,64]{1,4,3,2,0:T(8,128)(2,1)} %get-tuple-element.167, s32[]{:T(128)} %get-tuple-element.154), kind=kOutput, calls=%fused_computation.1.clone.1 | convolution fusion | flops 306706944 | bytes 10426880 | tf_op jit(solution)/shard_map/while/body/eval_jaxpr/qhcd,khcd->hcqk/dot_general | solution.py:75
  253.0 5.6 %fusion.55 = f32[2,2,384]{2,1,0:T(2,128)S(1)} fusion(f32[2,2,1536,384]{3,2,1,0:T(8,128)} %get-tuple-element.142, f32[2,2,384]{2,1,0:T(2,128)S(1)} %fusion.54), kind=kLoop, calls=%fused_computation.4.clone.1 | loop fusion | flops 7076352 | bytes 9449472 | tf_op jit(solution)/shard_map/while/body/eval_jaxpr/reduce_sum | solution.py:81
  258.7 1.6 constant_dynamic-slice_fusion.2
  260.3 2.6 fusion.57
  263.0 6.2 %bitcast_reduce_fusion.2 = (f32[2,2,384]{2,1,0:T(2,128)S(1)}, f32[2,2,1536,384]{3,2,1,0:T(8,128)}) fusion(bf16[384,2,2,64]{0,3,2,1:T(8,128)(2,1)S(1)} %get-tuple-element.168, bf16[8,1536,2,2,64]{1,4,3,2,0:T(8,128)(2,1)} %get-tuple-element.167, s32[]{:T(128)} %get-tuple-element.154), kind=kOutput, calls=%fused_computation.1.clone.1 | convolution fusion | flops 306706944 | bytes 10426880 | tf_op jit(solution)/shard_map/while/body/eval_jaxpr/qhcd,khcd->hcqk/dot_general | solution.py:75
  269.2 5.4 %fusion.55 = f32[2,2,384]{2,1,0:T(2,128)S(1)} fusion(f32[2,2,1536,384]{3,2,1,0:T(8,128)} %get-tuple-element.142, f32[2,2,384]{2,1,0:T(2,128)S(1)} %fusion.54), kind=kLoop, calls=%fused_computation.4.clone.1 | loop fusion | flops 7076352 | bytes 9449472 | tf_op jit(solution)/shard_map/while/body/eval_jaxpr/reduce_sum | solution.py:81
  274.7 1.6 constant_dynamic-slice_fusion.2
  276.3 2.6 fusion.57
  279.0 6.2 %bitcast_reduce_fusion.2 = (f32[2,2,384]{2,1,0:T(2,128)S(1)}, f32[2,2,1536,384]{3,2,1,0:T(8,128)}) fusion(bf16[384,2,2,64]{0,3,2,1:T(8,128)(2,1)S(1)} %get-tuple-element.168, bf16[8,1536,2,2,64]{1,4,3,2,0:T(8,128)(2,1)} %get-tuple-element.167, s32[]{:T(128)} %get-tuple-element.154), kind=kOutput, calls=%fused_computation.1.clone.1 | convolution fusion | flops 306706944 | bytes 10426880 | tf_op jit(solution)/shard_map/while/body/eval_jaxpr/qhcd,khcd->hcqk/dot_general | solution.py:75
  285.2 5.4 %fusion.55 = f32[2,2,384]{2,1,0:T(2,128)S(1)} fusion(f32[2,2,1536,384]{3,2,1,0:T(8,128)} %get-tuple-element.142, f32[2,2,384]{2,1,0:T(2,128)S(1)} %fusion.54), kind=kLoop, calls=%fused_computation.4.clone.1 | loop fusion | flops 7076352 | bytes 9449472 | tf_op jit(solution)/shard_map/while/body/eval_jaxpr/reduce_sum | solution.py:81
  290.6 1.6 constant_dynamic-slice_fusion.2
  292.2 2.6 fusion.57
  294.9 6.2 %bitcast_reduce_fusion.2 = (f32[2,2,384]{2,1,0:T(2,128)S(1)}, f32[2,2,1536,384]{3,2,1,0:T(8,128)}) fusion(bf16[384,2,2,64]{0,3,2,1:T(8,128)(2,1)S(1)} %get-tuple-element.168, bf16[8,1536,2,2,64]{1,4,3,2,0:T(8,128)(2,1)} %get-tuple-element.167, s32[]{:T(128)} %get-tuple-element.154), kind=kOutput, calls=%fused_computation.1.clone.1 | convolution fusion | flops 306706944 | bytes 10426880 | tf_op jit(solution)/shard_map/while/body/eval_jaxpr/qhcd,khcd->hcqk/dot_general | solution.py:75
  301.1 5.4 %fusion.55 = f32[2,2,384]{2,1,0:T(2,128)S(1)} fusion(f32[2,2,1536,384]{3,2,1,0:T(8,128)} %get-tuple-element.142, f32[2,2,384]{2,1,0:T(2,128)S(1)} %fusion.54), kind=kLoop, calls=%fused_computation.4.clone.1 | loop fusion | flops 7076352 | bytes 9449472 | tf_op jit(solution)/shard_map/while/body/eval_jaxpr/reduce_sum | solution.py:81
  306.5 1.6 constant_dynamic-slice_fusion.2
  308.1 2.6 fusion.57
  310.8 6.2 %bitcast_reduce_fusion.2 = (f32[2,2,384]{2,1,0:T(2,128)S(1)}, f32[2,2,1536,384]{3,2,1,0:T(8,128)}) fusion(bf16[384,2,2,64]{0,3,2,1:T(8,128)(2,1)S(1)} %get-tuple-element.168, bf16[8,1536,2,2,64]{1,4,3,2,0:T(8,128)(2,1)} %get-tuple-element.167, s32[]{:T(128)} %get-tuple-element.154), kind=kOutput, calls=%fused_computation.1.clone.1 | convolution fusion | flops 306706944 | bytes 10426880 | tf_op jit(solution)/shard_map/while/body/eval_jaxpr/qhcd,khcd->hcqk/dot_general | solution.py:75
  317.0 5.4 %fusion.55 = f32[2,2,384]{2,1,0:T(2,128)S(1)} fusion(f32[2,2,1536,384]{3,2,1,0:T(8,128)} %get-tuple-element.142, f32[2,2,384]{2,1,0:T(2,128)S(1)} %fusion.54), kind=kLoop, calls=%fused_computation.4.clone.1 | loop fusion | flops 7076352 | bytes 9449472 | tf_op jit(solution)/shard_map/while/body/eval_jaxpr/reduce_sum | solution.py:81
  322.4 1.6 constant_dynamic-slice_fusion.2
  324.0 2.6 fusion.57
  328.3 26.4 %all_to_all.15 = bf16[8,48,2048]{2,1,0:T(8,128)(2,1)S(1)} all-to-all(bf16[8,48,2048]{2,1,0:T(8,128)(2,1)S(1)} %bitcast.67), channel_id=1, replica_groups=mesh['sp'=32,'tp'=8] {'tp'}, dimensions={0} | all-to-all | bytes 3145728 | tf_op jit(solution)/shard_map/all_to_all | solution.py:19
  355.4 24.0 %all_to_all.16 = bf16[8,48,2048]{2,1,0:T(8,128)(2,1)S(1)} all-to-all(bf16[8,48,2048]{2,1,0:T(8,128)(2,1)S(1)} %broadcast_in_dim.13), channel_id=1, replica_groups=mesh['sp'=32,'tp'=8] {'tp'}, dimensions={0} | all-to-all | bytes 3145728 | tf_op jit(solution)/shard_map/all_to_all | solution.py:25
  379.5 4.6 %fusion.21 = f32[384,704]{0,1:T(8,128)} fusion(bf16[384,2048]{1,0:T(8,128)(2,1)S(1)} %bitcast.68, bf16[2048,2112]{1,0:T(8,128)(2,1)} %all-gather.8.cloned.1.call-done), kind=kOutput, calls=%fused_computation.26 | convolution fusion | flops 1107296256 | bytes 5799936 | tf_op jit(solution)/shard_map/dot_general | solution.py:125
  384.0 8.8 %fusion.23 = bf16[384,2048]{1,0:T(8,128)(2,1)} fusion(bf16[2048,2112]{1,0:T(8,128)(2,1)} %all-gather.8.cloned.1.call-done, bf16[384,2048]{1,0:T(8,128)(2,1)S(1)} %bitcast.69, f32[384,704]{0,1:T(8,128)} %fusion.21), kind=kOutput, calls=%fused_computation.30 | convolution fusion | flops 2217000960 | bytes 10518528 | tf_op jit(solution)/shard_map/dot_general | solution.py:130
  392.8 25.1 %all_to_all.17 = bf16[8,48,2048]{2,1,0:T(8,128)(2,1)S(1)} all-to-all(bf16[8,48,2048]{2,1,0:T(8,128)(2,1)} %bitcast.70), channel_id=1, replica_groups=mesh['sp'=32,'tp'=8] {'tp'}, dimensions={0} | all-to-all | bytes 3145728 | tf_op jit(solution)/shard_map/all_to_all | solution.py:19
  418.1 0.8 add_convert_fusion
  (71 shorter events, 2.8 us)
Async XLA Ops:
  6.5 321.1 %copy-start = (bf16[256,2048]{1,0:T(8,128)(2,1)S(1)}, bf16[256,2048]{1,0:T(8,128)(2,1)}, u32[]{:S(2)}) copy-start(bf16[256,2048]{1,0:T(8,128)(2,1)} %param.19) | copy-start | bytes 3145732
  6.5 94.5 %all-gather.4.cloned.1.call-start = ((), (), s32[]{:S(2)}) async-start(), calls=%async_computation.3 | async-start | bytes 6488064 | tf_op jit(solution)/shard_map/all_gather | solution.py:95
  7.3 181.5 %all-gather.6.cloned.1.call-start = ((), (), s32[]{:S(2)}) async-start(), calls=%async_computation.4 | async-start | bytes 6488064 | tf_op jit(solution)/shard_map/all_gather | solution.py:96
  8.0 371.5 %all-gather.8.cloned.1.call-start = ((), (), s32[]{:S(2)}) async-start(), calls=%async_computation.5 | async-start | bytes 9191424 | tf_op jit(solution)/shard_map/all_gather | solution.py:43
  204.7 7.1 %copy-start.1 = (f32[2,2,1536,384]{3,2,1,0:T(8,128)S(1)}, f32[2,2,1536,384]{3,2,1,0:T(8,128)}, u32[]{:S(2)}) copy-start(f32[2,2,1536,384]{3,2,1,0:T(8,128)} %get-tuple-element.142) | copy-start | bytes 28311556 | tf_op jit(solution)/shard_map/while
  220.7 7.1 %copy-start.1 = (f32[2,2,1536,384]{3,2,1,0:T(8,128)S(1)}, f32[2,2,1536,384]{3,2,1,0:T(8,128)}, u32[]{:S(2)}) copy-start(f32[2,2,1536,384]{3,2,1,0:T(8,128)} %get-tuple-element.142) | copy-start | bytes 28311556 | tf_op jit(solution)/shard_map/while
  236.6 7.5 %copy-start.1 = (f32[2,2,1536,384]{3,2,1,0:T(8,128)S(1)}, f32[2,2,1536,384]{3,2,1,0:T(8,128)}, u32[]{:S(2)}) copy-start(f32[2,2,1536,384]{3,2,1,0:T(8,128)} %get-tuple-element.142) | copy-start | bytes 28311556 | tf_op jit(solution)/shard_map/while
  253.0 7.3 %copy-start.1 = (f32[2,2,1536,384]{3,2,1,0:T(8,128)S(1)}, f32[2,2,1536,384]{3,2,1,0:T(8,128)}, u32[]{:S(2)}) copy-start(f32[2,2,1536,384]{3,2,1,0:T(8,128)} %get-tuple-element.142) | copy-start | bytes 28311556 | tf_op jit(solution)/shard_map/while
  269.2 7.1 %copy-start.1 = (f32[2,2,1536,384]{3,2,1,0:T(8,128)S(1)}, f32[2,2,1536,384]{3,2,1,0:T(8,128)}, u32[]{:S(2)}) copy-start(f32[2,2,1536,384]{3,2,1,0:T(8,128)} %get-tuple-element.142) | copy-start | bytes 28311556 | tf_op jit(solution)/shard_map/while
  285.2 7.0 %copy-start.1 = (f32[2,2,1536,384]{3,2,1,0:T(8,128)S(1)}, f32[2,2,1536,384]{3,2,1,0:T(8,128)}, u32[]{:S(2)}) copy-start(f32[2,2,1536,384]{3,2,1,0:T(8,128)} %get-tuple-element.142) | copy-start | bytes 28311556 | tf_op jit(solution)/shard_map/while
  301.1 7.0 %copy-start.1 = (f32[2,2,1536,384]{3,2,1,0:T(8,128)S(1)}, f32[2,2,1536,384]{3,2,1,0:T(8,128)}, u32[]{:S(2)}) copy-start(f32[2,2,1536,384]{3,2,1,0:T(8,128)} %get-tuple-element.142) | copy-start | bytes 28311556 | tf_op jit(solution)/shard_map/while
  317.0 7.0 %copy-start.1 = (f32[2,2,1536,384]{3,2,1,0:T(8,128)S(1)}, f32[2,2,1536,384]{3,2,1,0:T(8,128)}, u32[]{:S(2)}) copy-start(f32[2,2,1536,384]{3,2,1,0:T(8,128)} %get-tuple-element.142) | copy-start | bytes 28311556 | tf_op jit(solution)/shard_map/while
  326.7 0.7 copy-start.4
  326.7 0.8 copy-start.5
  328.3 26.7 %copy-start.2 = (bf16[48,2048]{1,0:T(8,128)(2,1)S(1)}, bf16[48,2048]{1,0:T(8,128)(2,1)}, u32[]{:S(2)}) copy-start(bf16[48,2048]{1,0:T(8,128)(2,1)} %param.13) | copy-start | bytes 589828
  328.3 26.8 %copy-start.3 = (f32[2048]{0:T(1024)S(1)}, f32[2048]{0:T(1024)}, u32[]{:S(2)}) copy-start(f32[2048]{0:T(1024)} %param.20) | copy-start | bytes 24580
Sparse Core Ops, SparseCore 0:
  9.9 91.0 all-gather.3
  103.6 85.0 all-gather.5
  191.3 97.5 all-gather.7
where the time goes:
time: 428 us; the launch traced here: 425 us
  waiting for transfers between devices  127 us (30%)
  matrix products  84.7 us (20%)
  local copies, waits for them, and re-layouts  78.1 us (18%)
  blocking collectives  75.5 us (18%)
  other arithmetic  45.7 us (11%)
  between operations  13.3 us (3%)
    all_gather x1, waiting for transfers between devices, body(): key_piece = lax.all_gather(keys, 'sp', axis=0, tiled=True)  89.9 us
    all_to_all x2, blocking collectives, sent_and_summed(): lax.all_to_all(parts, axis, split_axis=0, concat_axis=0, tiled=True)  51.5 us
    dot_general x8, matrix products, one_block(): jnp.einsum('qhcd,khcd->hcqk', query_four, key_block, preferred_element_ty...  49.6 us
    reduce_sum x8, other arithmetic, one_block(): total = total * rescale + jnp.sum(expo, axis=-1)  43.7 us
    all_gather x1, waiting for transfers between devices, body(): value_piece = lax.all_gather(values, 'sp', axis=0, tiled=True)  36.1 us
    unnamed x12, local copies, waits for them, and re-layouts  31.2 us
    all_to_all x1, blocking collectives, sent_to_all(): return lax.all_to_all(copies, axis, split_axis=0, concat_axis=0, tiled=True)  24 us
    reshape x1, local copies, waits for them, and re-layouts, body(): key_blocks = key_piece.reshape(blocks, width, heads_local, 2, DH)  21.8 us
  transfers between devices with their start and end apart: 3, of which 2 were waited for; matrix products, arithmetic and copies ran while one was open for 46% of the time, Pallas kernels for 0%

commit v1 on v0

--- a/solution.py
+++ b/solution.py
@@ -92,7 +92,8 @@
         jnp.zeros((heads_local, 2, tok_local), jnp.float32),
         jnp.zeros((heads_local, 2, tok_local, VD), jnp.float32),
     )
-    key_piece = lax.all_gather(keys, "sp", axis=0, tiled=True)
+    copies_2 = jnp.concatenate([keys] * lax.axis_size("sp"), axis=0)
+    key_piece = lax.all_to_all(copies_2, "sp", 0, 0, tiled=True)
     value_piece = lax.all_gather(values, "sp", axis=0, tiled=True)
     count = key_piece.shape[0]
     shards = max(count // tok_local, 1)

time: 428 us -> 489 us (1.14)
  waiting for transfers between devices: 127 us -> 176 us
  starting transfers between devices: 0.08 us -> 12.3 us
    all_to_all x0 -> x1, waiting for transfers between devices: none -> 175 us  [body(): key_piece = lax.all_to_all(copies_2, 'sp', 0, 0, tiled=True)]
    all_gather x1 -> x0, waiting for transfers between devices: 89.9 us -> none  [body(): key_piece = lax.all_gather(keys, 'sp', axis=0, tiled=True)]
    all_gather x1, waiting for transfers between devices: 36.1 us -> 0.01 us  [body(): value_piece = lax.all_gather(values, 'sp', axis=0, tiled=True)]
    all_to_all x0 -> x2, local copies, waits for them, and re-layouts: none -> 17.8 us  [body(): key_piece = lax.all_to_all(copies_2, 'sp', 0, 0, tiled=True)]
    all_to_all x0 -> x1, starting transfers between devices: none -> 12.3 us  [body(): key_piece = lax.all_to_all(copies_2, 'sp', 0, 0, tiled=True)]
    reshape x1, local copies, waits for them, and re-layouts: 21.8 us -> 10.7 us  [body(): key_blocks = key_piece.reshape(blocks, width, heads_local, 2, DH)]
    unnamed x12 -> x55, local copies, waits for them, and re-layouts: 31.2 us -> 26.1 us
  transfers between devices with their start and end apart: 3 -> 3, of which waited for: 2 -> 1; matrix products, arithmetic and copies ran while one was open for 46% -> 39% of each run, Pallas kernels for 0% -> 0%
where the time goes in v1:
time: 489 us; the launch traced here: 487 us
  waiting for transfers between devices  176 us (36%)
  matrix products  84.2 us (17%)
  local copies, waits for them, and re-layouts  78.5 us (16%)
  blocking collectives  76.9 us (16%)
  other arithmetic  45.4 us (9%)
  between operations  13.8 us (3%)
  starting transfers between devices  12.3 us (3%)
    all_to_all x1, waiting for transfers between devices, body(): key_piece = lax.all_to_all(copies_2, 'sp', 0, 0, tiled=True)  175 us
    all_to_all x2, blocking collectives, sent_and_summed(): lax.all_to_all(parts, axis, split_axis=0, concat_axis=0, tiled=True)  52.2 us
    dot_general x8, matrix products, one_block(): jnp.einsum('qhcd,khcd->hcqk', query_four, key_block, preferred_element_ty...  49.5 us
    reduce_sum x8, other arithmetic, one_block(): total = total * rescale + jnp.sum(expo, axis=-1)  43.4 us
    unnamed x55, local copies, waits for them, and re-layouts  26.1 us
    all_to_all x1, blocking collectives, sent_to_all(): return lax.all_to_all(copies, axis, split_axis=0, concat_axis=0, tiled=True)  24.7 us
    dot_general x8, matrix products, one_block(): jnp.einsum('hcqk,khe->hcqe', expo.astype(jnp.bfloat16), value_block, pref...  21.2 us
    all_to_all x2, local copies, waits for them, and re-layouts, body(): key_piece = lax.all_to_all(copies_2, 'sp', 0, 0, tiled=True)  17.8 us
  transfers between devices with their start and end apart: 3, of which 1 were waited for; matrix products, arithmetic and copies ran while one was open for 39% of the time, Pallas kernels for 0%

profile of v1, /device:TPU:1, one launch (start us, length us, event | category | flops | bytes accessed | tf_op | source)
XLA Modules:
  0.0 487.4 jit_solution(12614421456332718405)
XLA Ops:
  8.2 0.9 constant_dynamic-update-slice_fusion.30
  10.1 0.9 constant_dynamic-update-slice_fusion.28
  22.8 2.6 copy-done.3
  25.4 8.6 %copy.32 = bf16[32,384,256]{1,2,0:T(8,128)(2,1)} copy(bf16[32,384,256]{2,1,0:T(8,128)(2,1)} %bitcast.70) | data formatting | bytes 12582912 | tf_op jit(solution)/shard_map/all_to_all | solution.py:96
  34.0 12.3 %all-to-all-start = ((bf16[32,384,256]{1,2,0:T(8,128)(2,1)}), bf16[32,384,256]{1,2,0:T(8,128)(2,1)}, u32[]{:S(2)}, u32[]{:S(2)}) async-start(bf16[32,384,256]{1,2,0:T(8,128)(2,1)} %copy.32), calls=%async_computation | async-start | bytes 12582912 | tf_op jit(solution)/shard_map/all_to_all | solution.py:96
  47.4 175.1 %all-to-all-done = bf16[32,384,256]{1,2,0:T(8,128)(2,1)} async-done(((bf16[32,384,256]{1,2,0:T(8,128)(2,1)}), bf16[32,384,256]{1,2,0:T(8,128)(2,1)}, u32[]{:S(2)}, u32[]{:S(2)}) %all-to-all-start) | async-done | bytes 6291488 | tf_op jit(solution)/shard_map/all_to_all | solution.py:96
  222.5 9.2 %copy.33 = bf16[32,384,256]{1,0,2:T(8,128)(2,1)} copy(bf16[32,384,256]{1,2,0:T(8,128)(2,1)} %all-to-all-done) | data formatting | bytes 12582912 | tf_op jit(solution)/shard_map/all_to_all | solution.py:96
  231.7 10.7 %reshape.46 = bf16[8,1536,2,2,64]{1,0,4,3,2:T(8,128)(2,1)} reshape(bf16[32,384,256]{1,0,2:T(8,128)(2,1)} %copy.33) | data formatting | bytes 12582912 | tf_op jit(solution)/shard_map/reshape | solution.py:106
  242.3 8.0 %copy.36 = bf16[8,1536,2,2,64]{1,4,3,2,0:T(8,128)(2,1)} copy(bf16[8,1536,2,2,64]{1,0,4,3,2:T(8,128)(2,1)} %reshape.46) | data formatting | bytes 12582912
  250.3 9.8 %reshape.54 = bf16[8,1536,2,128]{3,2,1,0:T(2,128)(2,1)} reshape(bf16[12288,256]{1,0:T(8,128)(2,1)} %all-gather.3.cloned.1.call-done) | data formatting | bytes 12582912 | tf_op jit(solution)/shard_map/reshape | solution.py:107
  260.1 127.6 %while.15 = (s32[]{:T(128)}, f32[2,2,384]{2,1,0:T(2,128)S(1)}, f32[2,2,384]{2,1,0:T(2,128)S(1)}, f32[2,2,384,128]{3,2,1,0:T(8,128)S(1)}, bf16[8,1536,2,2,64]{1,4...) while((s32[]{:T(128)}, f32[2,2,384]{2,1,0:T(2,128)S(1)}, ...), condition=%wide.region_3.4_spmd.clone, body=%wide.region_0.3_spmd.clone.sunk | while | flops 925441536 | bytes 71074440 | solution.py:108
  260.1 6.2 %bitcast_reduce_fusion.2 = (f32[2,2,384]{2,1,0:T(2,128)S(1)}, f32[2,2,1536,384]{3,2,1,0:T(8,128)}) fusion(bf16[384,2,2,64]{0,3,2,1:T(8,128)(2,1)S(1)} %get-tuple-element.182, bf16[8,1536,2,2,64]{1,4,3,2,0:T(8,128)(2,1)} %get-tuple-element.181, s32[]{:T(128)} %get-tuple-element.168), kind=kOutput, calls=%fused_computation.1.clone.1 | convolution fusion | flops 306706944 | bytes 10426880 | tf_op jit(solution)/shard_map/while/body/eval_jaxpr/qhcd,khcd->hcqk/dot_general | solution.py:75
  266.3 5.6 %fusion.55 = f32[2,2,384]{2,1,0:T(2,128)S(1)} fusion(f32[2,2,1536,384]{3,2,1,0:T(8,128)} %get-tuple-element.156, f32[2,2,384]{2,1,0:T(2,128)S(1)} %fusion.54), kind=kLoop, calls=%fused_computation.4.clone.1 | loop fusion | flops 7076352 | bytes 9449472 | tf_op jit(solution)/shard_map/while/body/eval_jaxpr/reduce_sum | solution.py:81
  271.9 1.7 constant_dynamic-slice_fusion.2
  273.7 2.6 fusion.57
  276.3 6.2 %bitcast_reduce_fusion.2 = (f32[2,2,384]{2,1,0:T(2,128)S(1)}, f32[2,2,1536,384]{3,2,1,0:T(8,128)}) fusion(bf16[384,2,2,64]{0,3,2,1:T(8,128)(2,1)S(1)} %get-tuple-element.182, bf16[8,1536,2,2,64]{1,4,3,2,0:T(8,128)(2,1)} %get-tuple-element.181, s32[]{:T(128)} %get-tuple-element.168), kind=kOutput, calls=%fused_computation.1.clone.1 | convolution fusion | flops 306706944 | bytes 10426880 | tf_op jit(solution)/shard_map/while/body/eval_jaxpr/qhcd,khcd->hcqk/dot_general | solution.py:75
  282.6 5.5 %fusion.55 = f32[2,2,384]{2,1,0:T(2,128)S(1)} fusion(f32[2,2,1536,384]{3,2,1,0:T(8,128)} %get-tuple-element.156, f32[2,2,384]{2,1,0:T(2,128)S(1)} %fusion.54), kind=kLoop, calls=%fused_computation.4.clone.1 | loop fusion | flops 7076352 | bytes 9449472 | tf_op jit(solution)/shard_map/while/body/eval_jaxpr/reduce_sum | solution.py:81
  288.1 1.6 constant_dynamic-slice_fusion.2
  289.7 2.6 fusion.57
  292.4 6.2 %bitcast_reduce_fusion.2 = (f32[2,2,384]{2,1,0:T(2,128)S(1)}, f32[2,2,1536,384]{3,2,1,0:T(8,128)}) fusion(bf16[384,2,2,64]{0,3,2,1:T(8,128)(2,1)S(1)} %get-tuple-element.182, bf16[8,1536,2,2,64]{1,4,3,2,0:T(8,128)(2,1)} %get-tuple-element.181, s32[]{:T(128)} %get-tuple-element.168), kind=kOutput, calls=%fused_computation.1.clone.1 | convolution fusion | flops 306706944 | bytes 10426880 | tf_op jit(solution)/shard_map/while/body/eval_jaxpr/qhcd,khcd->hcqk/dot_general | solution.py:75
  298.6 5.4 %fusion.55 = f32[2,2,384]{2,1,0:T(2,128)S(1)} fusion(f32[2,2,1536,384]{3,2,1,0:T(8,128)} %get-tuple-element.156, f32[2,2,384]{2,1,0:T(2,128)S(1)} %fusion.54), kind=kLoop, calls=%fused_computation.4.clone.1 | loop fusion | flops 7076352 | bytes 9449472 | tf_op jit(solution)/shard_map/while/body/eval_jaxpr/reduce_sum | solution.py:81
  304.0 1.6 constant_dynamic-slice_fusion.2
  305.6 2.6 fusion.57
  308.3 6.2 %bitcast_reduce_fusion.2 = (f32[2,2,384]{2,1,0:T(2,128)S(1)}, f32[2,2,1536,384]{3,2,1,0:T(8,128)}) fusion(bf16[384,2,2,64]{0,3,2,1:T(8,128)(2,1)S(1)} %get-tuple-element.182, bf16[8,1536,2,2,64]{1,4,3,2,0:T(8,128)(2,1)} %get-tuple-element.181, s32[]{:T(128)} %get-tuple-element.168), kind=kOutput, calls=%fused_computation.1.clone.1 | convolution fusion | flops 306706944 | bytes 10426880 | tf_op jit(solution)/shard_map/while/body/eval_jaxpr/qhcd,khcd->hcqk/dot_general | solution.py:75
  314.5 5.4 %fusion.55 = f32[2,2,384]{2,1,0:T(2,128)S(1)} fusion(f32[2,2,1536,384]{3,2,1,0:T(8,128)} %get-tuple-element.156, f32[2,2,384]{2,1,0:T(2,128)S(1)} %fusion.54), kind=kLoop, calls=%fused_computation.4.clone.1 | loop fusion | flops 7076352 | bytes 9449472 | tf_op jit(solution)/shard_map/while/body/eval_jaxpr/reduce_sum | solution.py:81
  319.9 1.6 constant_dynamic-slice_fusion.2
  321.5 2.6 fusion.57
  324.2 6.2 %bitcast_reduce_fusion.2 = (f32[2,2,384]{2,1,0:T(2,128)S(1)}, f32[2,2,1536,384]{3,2,1,0:T(8,128)}) fusion(bf16[384,2,2,64]{0,3,2,1:T(8,128)(2,1)S(1)} %get-tuple-element.182, bf16[8,1536,2,2,64]{1,4,3,2,0:T(8,128)(2,1)} %get-tuple-element.181, s32[]{:T(128)} %get-tuple-element.168), kind=kOutput, calls=%fused_computation.1.clone.1 | convolution fusion | flops 306706944 | bytes 10426880 | tf_op jit(solution)/shard_map/while/body/eval_jaxpr/qhcd,khcd->hcqk/dot_general | solution.py:75
  330.3 5.4 %fusion.55 = f32[2,2,384]{2,1,0:T(2,128)S(1)} fusion(f32[2,2,1536,384]{3,2,1,0:T(8,128)} %get-tuple-element.156, f32[2,2,384]{2,1,0:T(2,128)S(1)} %fusion.54), kind=kLoop, calls=%fused_computation.4.clone.1 | loop fusion | flops 7076352 | bytes 9449472 | tf_op jit(solution)/shard_map/while/body/eval_jaxpr/reduce_sum | solution.py:81
  335.8 1.6 constant_dynamic-slice_fusion.2
  337.4 2.6 fusion.57
  340.0 6.2 %bitcast_reduce_fusion.2 = (f32[2,2,384]{2,1,0:T(2,128)S(1)}, f32[2,2,1536,384]{3,2,1,0:T(8,128)}) fusion(bf16[384,2,2,64]{0,3,2,1:T(8,128)(2,1)S(1)} %get-tuple-element.182, bf16[8,1536,2,2,64]{1,4,3,2,0:T(8,128)(2,1)} %get-tuple-element.181, s32[]{:T(128)} %get-tuple-element.168), kind=kOutput, calls=%fused_computation.1.clone.1 | convolution fusion | flops 306706944 | bytes 10426880 | tf_op jit(solution)/shard_map/while/body/eval_jaxpr/qhcd,khcd->hcqk/dot_general | solution.py:75
  346.2 5.4 %fusion.55 = f32[2,2,384]{2,1,0:T(2,128)S(1)} fusion(f32[2,2,1536,384]{3,2,1,0:T(8,128)} %get-tuple-element.156, f32[2,2,384]{2,1,0:T(2,128)S(1)} %fusion.54), kind=kLoop, calls=%fused_computation.4.clone.1 | loop fusion | flops 7076352 | bytes 9449472 | tf_op jit(solution)/shard_map/while/body/eval_jaxpr/reduce_sum | solution.py:81
  351.6 1.6 constant_dynamic-slice_fusion.2
  353.2 2.6 fusion.57
  355.9 6.2 %bitcast_reduce_fusion.2 = (f32[2,2,384]{2,1,0:T(2,128)S(1)}, f32[2,2,1536,384]{3,2,1,0:T(8,128)}) fusion(bf16[384,2,2,64]{0,3,2,1:T(8,128)(2,1)S(1)} %get-tuple-element.182, bf16[8,1536,2,2,64]{1,4,3,2,0:T(8,128)(2,1)} %get-tuple-element.181, s32[]{:T(128)} %get-tuple-element.168), kind=kOutput, calls=%fused_computation.1.clone.1 | convolution fusion | flops 306706944 | bytes 10426880 | tf_op jit(solution)/shard_map/while/body/eval_jaxpr/qhcd,khcd->hcqk/dot_general | solution.py:75
  362.1 5.4 %fusion.55 = f32[2,2,384]{2,1,0:T(2,128)S(1)} fusion(f32[2,2,1536,384]{3,2,1,0:T(8,128)} %get-tuple-element.156, f32[2,2,384]{2,1,0:T(2,128)S(1)} %fusion.54), kind=kLoop, calls=%fused_computation.4.clone.1 | loop fusion | flops 7076352 | bytes 9449472 | tf_op jit(solution)/shard_map/while/body/eval_jaxpr/reduce_sum | solution.py:81
  367.5 1.6 constant_dynamic-slice_fusion.2
  369.1 2.6 fusion.57
  371.8 6.2 %bitcast_reduce_fusion.2 = (f32[2,2,384]{2,1,0:T(2,128)S(1)}, f32[2,2,1536,384]{3,2,1,0:T(8,128)}) fusion(bf16[384,2,2,64]{0,3,2,1:T(8,128)(2,1)S(1)} %get-tuple-element.182, bf16[8,1536,2,2,64]{1,4,3,2,0:T(8,128)(2,1)} %get-tuple-element.181, s32[]{:T(128)} %get-tuple-element.168), kind=kOutput, calls=%fused_computation.1.clone.1 | convolution fusion | flops 306706944 | bytes 10426880 | tf_op jit(solution)/shard_map/while/body/eval_jaxpr/qhcd,khcd->hcqk/dot_general | solution.py:75
  378.0 5.4 %fusion.55 = f32[2,2,384]{2,1,0:T(2,128)S(1)} fusion(f32[2,2,1536,384]{3,2,1,0:T(8,128)} %get-tuple-element.156, f32[2,2,384]{2,1,0:T(2,128)S(1)} %fusion.54), kind=kLoop, calls=%fused_computation.4.clone.1 | loop fusion | flops 7076352 | bytes 9449472 | tf_op jit(solution)/shard_map/while/body/eval_jaxpr/reduce_sum | solution.py:81
  383.4 1.6 constant_dynamic-slice_fusion.2
  385.0 2.6 fusion.57
  389.0 27.1 %all_to_all.24 = bf16[8,48,2048]{2,1,0:T(8,128)(2,1)S(1)} all-to-all(bf16[8,48,2048]{2,1,0:T(8,128)(2,1)S(1)} %bitcast.71), channel_id=1, replica_groups=mesh['sp'=32,'tp'=8] {'tp'}, dimensions={0} | all-to-all | bytes 3145728 | tf_op jit(solution)/shard_map/all_to_all | solution.py:19
  416.8 24.7 %all_to_all.25 = bf16[8,48,2048]{2,1,0:T(8,128)(2,1)} all-to-all(bf16[8,48,2048]{2,1,0:T(8,128)(2,1)S(1)} %broadcast_in_dim.13), channel_id=1, replica_groups=mesh['sp'=32,'tp'=8] {'tp'}, dimensions={0} | all-to-all | bytes 3145728 | tf_op jit(solution)/shard_map/all_to_all | solution.py:25
  441.5 4.1 fusion.21
  445.6 8.9 %fusion.23 = bf16[384,2048]{1,0:T(8,128)(2,1)} fusion(bf16[2048,2112]{1,0:T(8,128)(2,1)} %all-gather.5.cloned.1.call-done, bf16[384,2048]{1,0:T(8,128)(2,1)} %bitcast.73, f32[384,704]{0,1:T(8,128)S(1)} %fusion.21), kind=kOutput, calls=%fused_computation.30 | convolution fusion | flops 2217000960 | bytes 10518528 | tf_op jit(solution)/shard_map/dot_general | solution.py:131
  454.5 25.1 %all_to_all.26 = bf16[8,48,2048]{2,1,0:T(8,128)(2,1)S(1)} all-to-all(bf16[8,48,2048]{2,1,0:T(8,128)(2,1)} %bitcast.74), channel_id=1, replica_groups=mesh['sp'=32,'tp'=8] {'tp'}, dimensions={0} | all-to-all | bytes 3145728 | tf_op jit(solution)/shard_map/all_to_all | solution.py:19
  (116 shorter events, 18.4 us)
Async XLA Ops:
  6.5 381.8 %copy-start = (bf16[256,2048]{1,0:T(8,128)(2,1)S(1)}, bf16[256,2048]{1,0:T(8,128)(2,1)}, u32[]{:S(2)}) copy-start(bf16[256,2048]{1,0:T(8,128)(2,1)} %param.19) | copy-start | bytes 3145732
  6.5 15.9 %copy-start.2 = (bf16[384,256]{1,0:T(8,128)(2,1)S(1)}, bf16[384,256]{1,0:T(8,128)(2,1)}, u32[]{:S(2)}) copy-start(bf16[384,256]{1,0:T(8,128)(2,1)} %param.15) | copy-start | bytes 589828
  6.5 243.8 %all-gather.3.cloned.1.call-start = ((), (), s32[]{:S(2)}) async-start(), calls=%async_computation.4 | async-start | bytes 6488064 | tf_op jit(solution)/shard_map/all_gather | solution.py:97
  22.8 2.6 copy-start.3
  34.0 12.3 %copy-start.6 = (bf16[64,704]{1,0:T(8,128)(2,1)S(1)}, bf16[64,704]{1,0:T(8,128)(2,1)}, u32[]{:S(2)}) copy-start(bf16[64,704]{1,0:T(8,128)(2,1)} %param.21) | copy-start | bytes 270340
  34.0 12.3 %copy-start.7 = (bf16[64,704]{1,0:T(8,128)(2,1)S(1)}, bf16[64,704]{1,0:T(8,128)(2,1)}, u32[]{:S(2)}) copy-start(bf16[64,704]{1,0:T(8,128)(2,1)} %param.22) | copy-start | bytes 270340
  34.0 12.3 %copy-start.8 = (bf16[704,64]{0,1:T(8,128)(2,1)S(1)}, bf16[704,64]{0,1:T(8,128)(2,1)}, u32[]{:S(2)}) copy-start(bf16[704,64]{0,1:T(8,128)(2,1)} %param.23) | copy-start | bytes 270340
  34.0 13.2 %copy-start.5 = (bf16[384,256]{1,0:T(8,128)(2,1)S(1)}, bf16[384,256]{1,0:T(8,128)(2,1)}, u32[]{:S(2)}) copy-start(bf16[384,256]{1,0:T(8,128)(2,1)} %param.14) | copy-start | bytes 589828
  34.0 188.5 %all-to-all-start = ((bf16[32,384,256]{1,2,0:T(8,128)(2,1)}), bf16[32,384,256]{1,2,0:T(8,128)(2,1)}, u32[]{:S(2)}, u32[]{:S(2)}) async-start(bf16[32,384,256]{1,2,0:T(8,128)(2,1)} %copy.32), calls=%async_computation | async-start | bytes 12582912 | tf_op jit(solution)/shard_map/all_to_all | solution.py:96
  46.3 395.3 %all-gather.5.cloned.1.call-start = ((), (), s32[]{:S(2)}) async-start(), calls=%async_computation.5 | async-start | bytes 9191424 | tf_op jit(solution)/shard_map/all_gather | solution.py:43
  260.1 128.0 %copy-start.10 = (f32[2]{0:T(128)S(1)}, f32[2]{0:T(128)}, u32[]{:S(2)}) copy-start(f32[2]{0:T(128)} %param.17) | copy-start | bytes 28
  260.1 128.1 %copy-start.11 = (f32[128]{0:T(128)S(1)}, f32[128]{0:T(128)}, u32[]{:S(2)}) copy-start(f32[128]{0:T(128)} %param.18) | copy-start | bytes 1540
  266.3 7.3 %copy-start.1 = (f32[2,2,1536,384]{3,2,1,0:T(8,128)S(1)}, f32[2,2,1536,384]{3,2,1,0:T(8,128)}, u32[]{:S(2)}) copy-start(f32[2,2,1536,384]{3,2,1,0:T(8,128)} %get-tuple-element.156) | copy-start | bytes 28311556 | tf_op jit(solution)/shard_map/while
  282.5 7.1 %copy-start.1 = (f32[2,2,1536,384]{3,2,1,0:T(8,128)S(1)}, f32[2,2,1536,384]{3,2,1,0:T(8,128)}, u32[]{:S(2)}) copy-start(f32[2,2,1536,384]{3,2,1,0:T(8,128)} %get-tuple-element.156) | copy-start | bytes 28311556 | tf_op jit(solution)/shard_map/while
  298.6 7.0 %copy-start.1 = (f32[2,2,1536,384]{3,2,1,0:T(8,128)S(1)}, f32[2,2,1536,384]{3,2,1,0:T(8,128)}, u32[]{:S(2)}) copy-start(f32[2,2,1536,384]{3,2,1,0:T(8,128)} %get-tuple-element.156) | copy-start | bytes 28311556 | tf_op jit(solution)/shard_map/while
  314.5 7.0 %copy-start.1 = (f32[2,2,1536,384]{3,2,1,0:T(8,128)S(1)}, f32[2,2,1536,384]{3,2,1,0:T(8,128)}, u32[]{:S(2)}) copy-start(f32[2,2,1536,384]{3,2,1,0:T(8,128)} %get-tuple-element.156) | copy-start | bytes 28311556 | tf_op jit(solution)/shard_map/while
  330.3 7.0 %copy-start.1 = (f32[2,2,1536,384]{3,2,1,0:T(8,128)S(1)}, f32[2,2,1536,384]{3,2,1,0:T(8,128)}, u32[]{:S(2)}) copy-start(f32[2,2,1536,384]{3,2,1,0:T(8,128)} %get-tuple-element.156) | copy-start | bytes 28311556 | tf_op jit(solution)/shard_map/while
  346.2 7.0 %copy-start.1 = (f32[2,2,1536,384]{3,2,1,0:T(8,128)S(1)}, f32[2,2,1536,384]{3,2,1,0:T(8,128)}, u32[]{:S(2)}) copy-start(f32[2,2,1536,384]{3,2,1,0:T(8,128)} %get-tuple-element.156) | copy-start | bytes 28311556 | tf_op jit(solution)/shard_map/while
  362.1 7.0 %copy-start.1 = (f32[2,2,1536,384]{3,2,1,0:T(8,128)S(1)}, f32[2,2,1536,384]{3,2,1,0:T(8,128)}, u32[]{:S(2)}) copy-start(f32[2,2,1536,384]{3,2,1,0:T(8,128)} %get-tuple-element.156) | copy-start | bytes 28311556 | tf_op jit(solution)/shard_map/while
  378.0 7.0 %copy-start.1 = (f32[2,2,1536,384]{3,2,1,0:T(8,128)S(1)}, f32[2,2,1536,384]{3,2,1,0:T(8,128)}, u32[]{:S(2)}) copy-start(f32[2,2,1536,384]{3,2,1,0:T(8,128)} %get-tuple-element.156) | copy-start | bytes 28311556 | tf_op jit(solution)/shard_map/while
  387.7 28.6 %copy-start.4 = (bf16[48,2048]{1,0:T(8,128)(2,1)S(1)}, bf16[48,2048]{1,0:T(8,128)(2,1)}, u32[]{:S(2)}) copy-start(bf16[48,2048]{1,0:T(8,128)(2,1)} %param.13) | copy-start | bytes 589828
  388.0 28.5 %copy-start.9 = (f32[2048]{0:T(1024)S(1)}, f32[2048]{0:T(1024)}, u32[]{:S(2)}) copy-start(f32[2048]{0:T(1024)} %param.20) | copy-start | bytes 24580
Sparse Core Ops, SparseCore 0:
  9.9 168.3 all-gather.2
  180.8 111.7 all-gather.4
